TPU v7x, 32 devices: a whole 2x2x4 slice. The times are simulated.
32 devices in a mesh: ep: 8 (over z, x), tp: 4 (over y, core).
Axes of the slice: x: 2, y: 2, z: 4, core: 2. Of those that a mesh axis runs over, the one named last changes fastest.
Arguments:
- tokens: bfloat16 [4608, 2048], P(('ep', 'tp')), may hold values from -6 to 6
- norm_gain: float32 [2048], replicated, may hold values from 0.1 to 1.9
- expert_ids: int32 [4608, 8], P(('ep', 'tp')), may hold values from 0 to 15, all different within a row; in each aligned block of 144 rows (0 to 143, 144 to 287, ...) at most 144 rows name the same one
- route_weights: float32 [4608, 8], P(('ep', 'tp')), may hold values from 0.3 to 1
- expert_gate: bfloat16 [16, 512, 2048], P('ep', 'tp'), may hold values from -0.125 to 0.125
- expert_up: bfloat16 [16, 512, 2048], P('ep', 'tp'), may hold values from -0.125 to 0.125
- expert_down: bfloat16 [16, 512, 2048], P('ep', 'tp'), may hold values from -0.25 to 0.25
- shared_gate: bfloat16 [512, 2048], P('tp'), may hold values from -0.125 to 0.125
- shared_up: bfloat16 [512, 2048], P('tp'), may hold values from -0.125 to 0.125
- shared_down: bfloat16 [512, 2048], P('tp'), may hold values from -0.25 to 0.25
- side_in: bfloat16 [2048, 1024], P('ep'), may hold values from -0.125 to 0.125
- side_out: bfloat16 [2048, 1024], P('ep'), may hold values from -0.1875 to 0.1875
- side_gate: bfloat16 [2048], replicated, may hold values from -0.125 to 0.125
Outputs:
- mixed: bfloat16 [4608, 2048], P(('ep', 'tp'))
Inputs may be any that keep to these rules, and one draw needn't show every extreme that they name: `expert_ids`: each row names 8 different experts of 0 to 15; within the rows of one device (aligned blocks of 144 rows) no expert is named more than 144 times, and in some of those blocks some expert is named exactly 144 times.
All inputs are finite; a program needn't handle non-finite values.
Results may differ from a plain program's by a relative error of at most 0.0068.
Values may be sent and summed in bfloat16 or wider, within the bound.
A program may use at most 320 MiB of HBM per device.

v0:
```python
import jax
import jax.numpy as jnp
from jax import lax
from jax.sharding import PartitionSpec as P

norm_eps = 1.0


def normalize(tokens, norm_gain):
    values = tokens.astype(jnp.float32)
    scale_inv = lax.rsqrt(jnp.mean(values * values, axis=-1, keepdims=True) + norm_eps)
    return (values * scale_inv * norm_gain).astype(jnp.bfloat16)


def swiglu(gate_part, up_part):
    return (jax.nn.silu(gate_part) * up_part).astype(jnp.bfloat16)


def body(
    tokens,
    norm_gain,
    expert_ids,
    route_weights,
    expert_gate,
    expert_up,
    expert_down,
    shared_gate,
    shared_up,
    shared_down,
    side_in,
    side_out,
    side_gate,
):
    normed = normalize(tokens, norm_gain)
    tok_count, width = normed.shape
    top_count = expert_ids.shape[1]
    groups = lax.axis_size("ep")
    local_experts = expert_gate.shape[0]
    experts_all = groups * local_experts
    capacity = 2 * tok_count * top_count // experts_all
    pair_count = tok_count * top_count
    flat_ids = expert_ids.reshape(pair_count)
    one_hot = (flat_ids[:, None] == jnp.arange(experts_all, dtype=jnp.int32)[None, :]).astype(
        jnp.int32
    )
    earlier = jnp.cumsum(one_hot, axis=0) - 1
    slot_of = jnp.sum(one_hot * earlier, axis=1)
    position = flat_ids * capacity + slot_of
    source_row = jnp.arange(pair_count, dtype=jnp.int32) // top_count
    buffers = (
        jnp.zeros((experts_all * capacity, width), jnp.bfloat16)
        .at[position]
        .set(normed[source_row])
    )
    buffers = buffers.reshape(groups, local_experts, capacity, width)
    received = lax.all_to_all(buffers, "ep", split_axis=0, concat_axis=0, tiled=True)
    gate_piece = lax.all_gather(expert_gate, "tp", axis=1, tiled=True)
    up_piece = lax.all_gather(expert_up, "tp", axis=1, tiled=True)
    down_piece = lax.all_gather(expert_down, "tp", axis=1, tiled=True)
    gate_part = jnp.einsum(
        "secd,efd->secf", received, gate_piece, preferred_element_type=jnp.float32
    )
    up_part = jnp.einsum("secd,efd->secf", received, up_piece, preferred_element_type=jnp.float32)
    hidden = swiglu(gate_part, up_part)
    total = jnp.einsum("secf,efd->secd", hidden, down_piece, preferred_element_type=jnp.float32)
    returned = lax.all_to_all(
        total.astype(jnp.bfloat16), "ep", split_axis=0, concat_axis=0, tiled=True
    )
    picked = returned.reshape(experts_all * capacity, width)[position]
    weighted = picked.astype(jnp.float32) * route_weights.reshape(pair_count, 1)
    routed = jnp.sum(weighted.reshape(tok_count, top_count, width), axis=1)
    gate_piece = lax.all_gather(shared_gate, "tp", axis=0, tiled=True)
    up_piece = lax.all_gather(shared_up, "tp", axis=0, tiled=True)
    down_piece = lax.all_gather(shared_down, "tp", axis=0, tiled=True)
    gate_part = jnp.einsum("td,fd->tf", normed, gate_piece, preferred_element_type=jnp.float32)
    up_part = jnp.einsum("td,fd->tf", normed, up_piece, preferred_element_type=jnp.float32)
    hidden = swiglu(gate_part, up_part)
    shared = jnp.dot(hidden, down_piece, preferred_element_type=jnp.float32)
    whole_in, whole_out = (
        lax.all_gather(side_in, "ep", axis=0, tiled=True),
        lax.all_gather(side_out, "ep", axis=0, tiled=True),
    )
    side_hidden = jax.nn.silu(jnp.dot(normed, whole_in, preferred_element_type=jnp.float32)).astype(
        jnp.bfloat16
    )
    side_value = jnp.einsum("ts,ds->td", side_hidden, whole_out, preferred_element_type=jnp.float32)
    opening = jax.nn.sigmoid(jnp.dot(normed, side_gate, preferred_element_type=jnp.float32))
    return (routed + shared + opening[:, None] * side_value).astype(jnp.bfloat16)


def solution(mesh):
    placed = (
        P(("ep", "tp"), None),
        P(),
        P(("ep", "tp"), None),
        P(("ep", "tp"), None),
        P("ep", "tp", None),
        P("ep", "tp", None),
        P("ep", "tp", None),
        P("tp", None),
        P("tp", None),
        P("tp", None),
        P("ep", None),
        P("ep", None),
        P(),
    )
    return jax.shard_map(
        body, mesh=mesh, in_specs=placed, out_specs=P(("ep", "tp"), None), check_vma=False
    )
```

profile of v0, /device:TPU:0, one launch (start us, length us, event | category | flops | bytes accessed | tf_op | source)
XLA Modules:
  0.0 640.6 jit_solution(15951848686888456871)
XLA Ops:
  6.5 0.0 copy-start
  6.5 0.0 all-gather.11.cloned.1.call-start
  6.5 0.7 all-gather.11.cloned.1.call-update
  7.3 0.0 all-gather.9.cloned.1.call-start
  7.3 0.7 all-gather.9.cloned.1.call-update
  8.0 0.8 copy.22
  8.8 0.1 eq.29
  8.9 0.1 eq.25
  9.0 4.6 reduce-window.6
  13.6 0.4 slice_reduce_fusion
  14.0 0.2 reduce-window.9
  14.2 0.7 broadcast_multiply_fusion
  14.9 0.1 copy.21
  15.0 0.1 mul.71
  15.2 0.1 add_add_fusion
  15.4 1.3 fusion.21
  16.6 0.0 copy-done
  16.6 0.9 fusion.23
  17.5 35.8 %scatter_custom_fusion = bf16[2304,2048]{1,0:T(8,128)(2,1)} fusion(s32[1152]{0:T(1024)S(1)} %fusion.35, bf16[144,2048]{1,0:T(8,128)(2,1)S(1)} %fusion.23, s32[2048]{0:T(1024)S(1)} %pad_clamp_fusion.1, bf16[]{:T(256)} %constant.35.clone.1), kind=kCustom, calls=%fused_computation.17 | custom fusion | bytes 9437186 | tf_op jit(solution)/shard_map/scatter | solution.py:53
  53.3 7.3 %all-to-all-start = ((bf16[8,2,144,2048]{3,2,1,0:T(8,128)(2,1)}), bf16[8,2,144,2048]{3,2,1,0:T(8,128)(2,1)}, u32[]{:S(2)}, u32[]{:S(2)}) async-start(bf16[8,2,144,2048]{3,2,1,0:T(8,128)(2,1)} %bitcast.67), calls=%async_computation | async-start | bytes 18874368 | tf_op jit(solution)/shard_map/all_to_all | solution.py:56
  60.7 0.0 all-gather.13.cloned.1.call-start
  60.7 0.7 all-gather.13.cloned.1.call-update
  61.4 0.0 all-gather.15.cloned.1.call-start
  61.4 0.5 all-gather.15.cloned.1.call-update
  62.0 0.0 all-gather.17.cloned.1.call-start
  62.0 0.5 all-gather.17.cloned.1.call-update
  62.5 0.0 all-gather.19.cloned.1.call-start
  62.6 0.5 all-gather.19.cloned.1.call-update
  63.1 0.0 all-gather.11.cloned.1.call-done
  63.2 203.1 %all-to-all-done = bf16[8,2,144,2048]{3,2,1,0:T(8,128)(2,1)} async-done(((bf16[8,2,144,2048]{3,2,1,0:T(8,128)(2,1)}), bf16[8,2,144,2048]{3,2,1,0:T(8,128)(2,1)}, u32[]{:S(2)}, u32[]{:S(2)}) %all-to-all-start) | async-done | bytes 9437216 | tf_op jit(solution)/shard_map/all_to_all | solution.py:56
  266.3 10.3 %fusion.1 = f32[2,8,144,512]{3,2,1,0:T(8,128)} fusion(bf16[8,2,144,2048]{3,2,1,0:T(8,128)(2,1)} %all-to-all-done, bf16[2,512,2048]{2,1,0:T(8,128)(2,1)} %all-gather.11.cloned.1.call-done), kind=kOutput, calls=%fused_computation.6 | convolution fusion | flops 4831838208 | bytes 18350080 | tf_op jit(solution)/shard_map/secd,efd->secf/dot_general | solution.py:63
  276.6 0.0 all-gather.9.cloned.1.call-done
  276.6 10.2 %fusion.5 = bf16[8,2,144,512]{3,2,0,1:T(8,128)(2,1)S(1)} fusion(f32[2,8,144,512]{3,2,1,0:T(8,128)} %fusion.1, bf16[2,512,2048]{2,1,0:T(8,128)(2,1)} %all-gather.9.cloned.1.call-done, bf16[8,2,144,2048]{3,2,1,0:T(8,128)(2,1)} %all-to-all-done), kind=kOutput, calls=%fused_computation.11 | convolution fusion | flops 4838916096 | bytes 20709376 | tf_op jit(solution)/shard_map/secd,efd->secf/dot_general | solution.py:60
  286.8 0.0 all-gather.13.cloned.1.call-done
  286.8 9.6 %convert_bitcast_fusion = bf16[8,2,144,2048]{3,2,0,1:T(8,128)(2,1)} fusion(bf16[8,2,144,512]{3,2,0,1:T(8,128)(2,1)S(1)} %fusion.5, bf16[2,512,2048]{2,1,0:T(8,128)(2,1)} %all-gather.13.cloned.1.call-done), kind=kOutput, calls=%fused_computation.5 | convolution fusion | flops 4836556800 | bytes 15990784 | tf_op jit(solution)/shard_map/secf,efd->secd/dot_general | solution.py:65
  296.5 9.3 %copy.26 = bf16[8,2,144,2048]{3,2,1,0:T(8,128)(2,1)} copy(bf16[8,2,144,2048]{3,2,0,1:T(8,128)(2,1)} %convert_bitcast_fusion) | data formatting | bytes 18874368 | tf_op jit(solution)/shard_map/convert_element_type | solution.py:67
  305.7 0.0 copy-start.1
  305.7 0.0 copy-start.2
  305.7 5.2 all-to-all-start.1
  310.9 0.0 all-gather.21.cloned.1.call-start
  310.9 0.7 all-gather.21.cloned.1.call-update
  311.7 0.3 all-gather.23.cloned.1.call-start
  311.9 0.4 all-gather.23.cloned.1.call-update
  312.4 0.0 copy-done.1
  312.4 0.1 copy.27
  312.5 0.0 copy-done.2
  312.6 0.3 fusion.42
  312.8 0.0 all-gather.15.cloned.1.call-done
  312.8 2.4 fusion.41
  315.3 267.8 %all-to-all-done.1 = bf16[8,2,144,2048]{3,2,1,0:T(8,128)(2,1)} async-done(((bf16[8,2,144,2048]{3,2,1,0:T(8,128)(2,1)}), bf16[8,2,144,2048]{3,2,1,0:T(8,128)(2,1)}, u32[]{:S(2)}, u32[]{:S(2)}) %all-to-all-start.1) | async-done | bytes 9437216 | tf_op jit(solution)/shard_map/all_to_all | solution.py:66
  583.0 15.5 %gather_fusion = bf16[1152,2048]{1,0:T(8,128)(2,1)} fusion(bf16[2304,2048]{1,0:T(8,128)(2,1)} %bitcast.11, s32[2048]{0:T(1024)S(1)} %pad_clamp_fusion), kind=kCustom, calls=%fused_computation.1 | custom fusion | bytes 9441792 | tf_op jit(solution)/shard_map/gather | solution.py:69
  598.6 7.0 %fusion = f32[144,2048]{1,0:T(8,128)S(1)} fusion(bf16[1152,2048]{1,0:T(8,128)(2,1)} %gather_fusion, f32[144,8]{1,0:T(8,128)S(1)} %copy.27), kind=kLoop, calls=%fused_computation.4 | loop fusion | flops 6782976 | bytes 5902848 | tf_op jit(solution)/shard_map/reduce_sum | solution.py:71
  605.6 0.0 all-gather.17.cloned.1.call-done
  605.6 0.0 all-gather.19.cloned.1.call-done
  605.7 3.5 convolution_add_fusion
  609.2 0.0 all-gather.21.cloned.1.call-done
  609.2 17.7 %all-gather.23.cloned.1.call-done = bf16[2048,1024]{1,0:T(8,128)(2,1)} async-done(((bf16[256,1024]{1,0:T(8,128)(2,1)}), bf16[2048,1024]{1,0:T(8,128)(2,1)}) %all-gather.23.cloned.1.call-update) | async-done | bytes 4194320 | tf_op jit(solution)/shard_map/all_gather | solution.py:81
  626.9 6.5 %fusion.16 = bf16[144,2048]{1,0:T(8,128)(2,1)} fusion(f32[144,2048]{1,0:T(8,128)S(1)} %convolution_add_fusion, bf16[2048,1024]{1,0:T(8,128)(2,1)} %all-gather.23.cloned.1.call-done, f32[144]{0:T(256)S(1)} %add_divide_fusion, bf16[144,2048]{1,0:T(8,128)(2,1)S(1)} %fusion.23, bf16[2048,1024]{1,0:T(8,128)(2,1)} %all-gather.21.cloned.1.call-done), kind=kOutput, calls=%fused_computation.26 | convolution fusion | flops 1209581568 | bytes 10748480 | tf_op jit(solution)/shard_map/ts,ds->td/dot_general | solution.py:86
  (9 shorter events, 0.2 us)
Async XLA Ops:
  6.5 10.1 %copy-start = (bf16[144,2048]{1,0:T(8,128)(2,1)S(1)}, bf16[144,2048]{1,0:T(8,128)(2,1)}, u32[]{:S(2)}) copy-start(bf16[144,2048]{1,0:T(8,128)(2,1)} %param.13) | copy-start | bytes 1769476
  6.5 56.6 %all-gather.11.cloned.1.call-start = ((), (), s32[]{:S(2)}) async-start(), calls=%async_computation.3 | async-start | bytes 5242880 | tf_op jit(solution)/shard_map/all_gather | solution.py:58
  7.3 269.4 %all-gather.9.cloned.1.call-start = ((), (), s32[]{:S(2)}) async-start(), calls=%async_computation.2 | async-start | bytes 5242880 | tf_op jit(solution)/shard_map/all_gather | solution.py:57
  53.3 213.0 %all-to-all-start = ((bf16[8,2,144,2048]{3,2,1,0:T(8,128)(2,1)}), bf16[8,2,144,2048]{3,2,1,0:T(8,128)(2,1)}, u32[]{:S(2)}, u32[]{:S(2)}) async-start(bf16[8,2,144,2048]{3,2,1,0:T(8,128)(2,1)} %bitcast.67), calls=%async_computation | async-start | bytes 18874368 | tf_op jit(solution)/shard_map/all_to_all | solution.py:56
  60.7 226.2 %all-gather.13.cloned.1.call-start = ((), (), s32[]{:S(2)}) async-start(), calls=%async_computation.4 | async-start | bytes 5242880 | tf_op jit(solution)/shard_map/all_gather | solution.py:59
  61.4 251.5 %all-gather.15.cloned.1.call-start = ((), (), s32[]{:S(2)}) async-start(), calls=%async_computation.5 | async-start | bytes 2621440 | tf_op jit(solution)/shard_map/all_gather | solution.py:72
  62.0 543.7 %all-gather.17.cloned.1.call-start = ((), (), s32[]{:S(2)}) async-start(), calls=%async_computation.6 | async-start | bytes 2621440 | tf_op jit(solution)/shard_map/all_gather | solution.py:73
  62.5 543.1 %all-gather.19.cloned.1.call-start = ((), (), s32[]{:S(2)}) async-start(), calls=%async_computation.7 | async-start | bytes 2621440 | tf_op jit(solution)/shard_map/all_gather | solution.py:74
  305.7 6.7 %copy-start.1 = (f32[144,8]{0,1:T(8,128)S(1)}, f32[144,8]{0,1:T(8,128)}, u32[]{:S(2)}) copy-start(f32[144,8]{0,1:T(8,128)} %param.16) | copy-start | bytes 13828
  305.7 6.8 %copy-start.2 = (bf16[2048]{0:T(1024)(128)(2,1)S(1)}, bf16[2048]{0:T(1024)(128)(2,1)}, u32[]{:S(2)}) copy-start(bf16[2048]{0:T(1024)(128)(2,1)} %param.25) | copy-start | bytes 12292
  305.7 277.3 %all-to-all-start.1 = ((bf16[8,2,144,2048]{3,2,1,0:T(8,128)(2,1)}), bf16[8,2,144,2048]{3,2,1,0:T(8,128)(2,1)}, u32[]{:S(2)}, u32[]{:S(2)}) async-start(bf16[8,2,144,2048]{3,2,1,0:T(8,128)(2,1)} %copy.26), calls=%async_computation.1 | async-start | bytes 18874368 | tf_op jit(solution)/shard_map/all_to_all | solution.py:66
  310.9 298.3 %all-gather.21.cloned.1.call-start = ((), (), s32[]{:S(2)}) async-start(), calls=%async_computation.8 | async-start | bytes 4718592 | tf_op jit(solution)/shard_map/all_gather | solution.py:80
  311.7 315.3 %all-gather.23.cloned.1.call-start = ((), (), s32[]{:S(2)}) async-start(), calls=%async_computation.9 | async-start | bytes 4718592 | tf_op jit(solution)/shard_map/all_gather | solution.py:81
Sparse Core Ops, SparseCore 0:
  8.9 37.1 all-gather.10
  47.7 34.4 all-gather.8
  83.7 34.4 all-gather.12
  119.7 22.5 all-gather.14
  143.7 22.5 all-gather.16
  167.7 22.5 all-gather.18
  313.8 219.9 all-gather.20
  536.0 90.8 all-gather.22
where the time goes:
time: 644 us; the launch traced here: 641 us
  waiting for transfers between devices  494 us (77%)
  local copies, waits for them, and re-layouts  62.3 us (10%)
  matrix products  42.8 us (7%)
  other arithmetic  14.8 us (2%)
  between operations  14.1 us (2%)
  starting transfers between devices  13 us (2%)
    all_to_all x1, waiting for transfers between devices, body(): lax.all_to_all(total.astype(jnp.bfloat16), 'ep', split_axis=0, concat_axi...  268 us
    all_to_all x1, waiting for transfers between devices, body(): lax.all_to_all(buffers, 'ep', split_axis=0, concat_axis=0, tiled=True)  203 us
    scatter x1, local copies, waits for them, and re-layouts, body(): buffers = jnp.zeros((experts_all * capacity, width), jnp.bfloat16).at[pos...  35.8 us
    all_gather x1, waiting for transfers between devices, body(): lax.all_gather(side_out, 'ep', axis=0, tiled=True)  17.7 us
    gather x1, local copies, waits for them, and re-layouts, body(): picked = returned.reshape(experts_all * capacity, width)[position]  15.5 us
  transfers between devices with their start and end apart: 10, of which 3 were waited for; matrix products, arithmetic and copies ran while one was open for 18% of the time, Pallas kernels for 0%

commit v1 on v0

v1 whole, which is shorter than its diff:
```python
import jax
import jax.numpy as jnp
from jax import lax
from jax.sharding import PartitionSpec as P

norm_eps = 1.0


def normalize(tokens, norm_gain):
    values = tokens.astype(jnp.float32)
    scale_inv = lax.rsqrt(jnp.mean(values * values, axis=-1, keepdims=True) + norm_eps)
    return (values * scale_inv * norm_gain).astype(jnp.bfloat16)


def body(
    tokens,
    norm_gain,
    expert_ids,
    route_weights,
    expert_gate,
    expert_up,
    expert_down,
    shared_gate,
    shared_up,
    shared_down,
    side_in,
    side_out,
    side_gate,
):
    normed = normalize(tokens, norm_gain)
    tok_count, width = normed.shape
    groups = lax.axis_size("ep")
    me = lax.axis_index("ep")
    local_experts, ff_part, _ = expert_gate.shape
    experts_all = groups * local_experts
    shared_rows = shared_gate.shape[0] // groups
    side_all = side_in.shape[1]
    side_cols = side_all // groups

    named = expert_ids[:, :, None] == jnp.arange(experts_all, dtype=jnp.int32)
    dense = jnp.sum(jnp.where(named, route_weights[:, :, None], 0.0), axis=1)
    opening = jax.nn.sigmoid(jnp.dot(normed, side_gate, preferred_element_type=jnp.float32))
    aux = jnp.concatenate([dense, opening[:, None]], axis=1)

    all_normed = lax.all_gather(normed, "ep", axis=0, tiled=True)
    all_aux = lax.all_gather(aux, "ep", axis=0, tiled=True)

    def pack(expert_part, shared_part):
        own = lax.dynamic_slice_in_dim(shared_part, me * shared_rows, shared_rows, 0)
        return jnp.concatenate([expert_part.reshape(local_experts * ff_part, width), own], axis=0)

    gate_all = lax.all_gather(pack(expert_gate, shared_gate), "tp", axis=0, tiled=True)
    up_all = lax.all_gather(pack(expert_up, shared_up), "tp", axis=0, tiled=True)
    down_all = lax.all_gather(pack(expert_down, shared_down), "tp", axis=0, tiled=True)

    rows = side_in.shape[0]
    both = jnp.stack([side_in, side_out]).reshape(2, rows, groups, side_cols)
    both = lax.all_to_all(both.transpose(2, 0, 1, 3), "ep", split_axis=0, concat_axis=0, tiled=True)
    in_part = both[:, 0].reshape(groups * rows, side_cols)
    out_part = both[:, 1].reshape(groups * rows, side_cols)

    mine = lax.dynamic_slice_in_dim(all_aux, me * local_experts, local_experts, 1)
    block = local_experts * ff_part + shared_rows
    place = jnp.arange(gate_all.shape[0], dtype=jnp.int32) % block // ff_part
    scale = jnp.ones((all_normed.shape[0], gate_all.shape[0]), jnp.float32)
    for e in range(local_experts):
        scale = jnp.where(place[None, :] == e, mine[:, e : e + 1], scale)

    gate_part = jnp.einsum("td,fd->tf", all_normed, gate_all, preferred_element_type=jnp.float32)
    up_part = jnp.einsum("td,fd->tf", all_normed, up_all, preferred_element_type=jnp.float32)
    hidden = (jax.nn.silu(gate_part) * up_part * scale).astype(jnp.bfloat16)
    side_hidden = jax.nn.silu(jnp.dot(all_normed, in_part, preferred_element_type=jnp.float32))
    side_hidden = (side_hidden * all_aux[:, experts_all:]).astype(jnp.bfloat16)
    total = jnp.dot(hidden, down_all, preferred_element_type=jnp.float32)
    total = total + jnp.einsum("ts,ds->td", side_hidden, out_part, preferred_element_type=jnp.float32)
    return lax.psum_scatter(total.astype(jnp.bfloat16), "ep", scatter_dimension=0, tiled=True)


def solution(mesh):
    placed = (
        P(("ep", "tp"), None),
        P(),
        P(("ep", "tp"), None),
        P(("ep", "tp"), None),
        P("ep", "tp", None),
        P("ep", "tp", None),
        P("ep", "tp", None),
        P("tp", None),
        P("tp", None),
        P("tp", None),
        P("ep", None),
        P("ep", None),
        P(),
    )
    return jax.shard_map(
        body, mesh=mesh, in_specs=placed, out_specs=P(("ep", "tp"), None), check_vma=False
    )
```

time: 644 us -> 344 us (0.53)
  waiting for transfers between devices: 494 us -> 214 us
  local copies, waits for them, and re-layouts: 62.3 us -> 6.32 us
  blocking collectives: 0 us -> 46.5 us
  other arithmetic: 14.8 us -> 7.76 us
    all_to_all x2 -> x1, waiting for transfers between devices: 471 us -> 0.01 us  [body(): lax.all_to_all(both.transpose(2, 0, 1, 3), 'ep', split_axis=0, concat_axi...]
    all_gather x8 -> x4, waiting for transfers between devices: 17.9 us -> 118 us  [the longest x1 55.7 us: body(): all_normed = lax.all_gather(normed, 'ep', axis=0, tiled=True)]
    reduce_scatter x0 -> x1, waiting for transfers between devices: none -> 95.8 us  [body(): lax.psum_scatter(total.astype(jnp.bfloat16), 'ep', scatter_dimension=0, t...]
    all_gather x0 -> x1, blocking collectives: none -> 46.5 us  [body(): all_aux = lax.all_gather(aux, 'ep', axis=0, tiled=True)]
    scatter x1 -> x0, local copies, waits for them, and re-layouts: 35.8 us -> none  [body(): buffers = jnp.zeros((experts_all * capacity, width), jnp.bfloat16).at[pos...]
    gather x1 -> x0, local copies, waits for them, and re-layouts: 15.5 us -> none  [body(): picked = returned.reshape(experts_all * capacity, width)[position]]
    convert_element_type x1 -> x0, local copies, waits for them, and re-layouts: 9.26 us -> none  [body(): total.astype(jnp.bfloat16)]
    reduce_sum x2 -> x1, other arithmetic: 7.05 us -> 0.02 us  [body(): dense = jnp.sum(jnp.where(named, route_weights[:, :, None], 0.0), axis=1)]
  transfers between devices with their start and end apart: 10 -> 6, of which waited for: 3 -> 4; matrix products, arithmetic and copies ran while one was open for 18% -> 6% of each run, Pallas kernels for 0% -> 0%
where the time goes in v1:
time: 344 us; the launch traced here: 343 us
  waiting for transfers between devices  214 us (62%)
  matrix products  47.6 us (14%)
  blocking collectives  46.5 us (14%)
  between operations  13.3 us (4%)
  other arithmetic  7.76 us (2%)
  starting transfers between devices  7.49 us (2%)
  local copies, waits for them, and re-layouts  6.32 us (2%)
    reduce_scatter x1, waiting for transfers between devices, body(): lax.psum_scatter(total.astype(jnp.bfloat16), 'ep', scatter_dimension=0, t...  95.8 us
    all_gather x1, waiting for transfers between devices, body(): all_normed = lax.all_gather(normed, 'ep', axis=0, tiled=True)  55.7 us
    all_gather x1, blocking collectives, body(): all_aux = lax.all_gather(aux, 'ep', axis=0, tiled=True)  46.5 us
    all_gather x1, waiting for transfers between devices, body(): lax.all_gather(pack(expert_down, shared_down), 'tp', axis=0, tiled=True)  37.4 us
    dot_general x1, matrix products, body(): total = jnp.dot(hidden, down_all, preferred_element_type=jnp.float32)  25.3 us
    all_gather x1, waiting for transfers between devices, body(): lax.all_gather(pack(expert_up, shared_up), 'tp', axis=0, tiled=True)  25.2 us
    dot_general x1, matrix products, body(): jnp.einsum('ts,ds->td', side_hidden, out_part, preferred_element_type=jnp...  11.4 us
    dot_general x1, matrix products, body(): jnp.einsum('td,fd->tf', all_normed, gate_all, preferred_element_type=jnp....  10.7 us
  transfers between devices with their start and end apart: 6, of which 4 were waited for; matrix products, arithmetic and copies ran while one was open for 6% of the time, Pallas kernels for 0%

profile of v1, /device:TPU:0, one launch (start us, length us, event | category | flops | bytes accessed | tf_op | source)
XLA Modules:
  0.0 343.2 jit_solution(12004345322271529971)
XLA Ops:
  6.5 0.0 copy-start
  6.5 0.0 copy-start.2
  6.5 0.0 copy-start.3
  6.5 0.0 all-gather.8.cloned.1.call-start
  6.6 1.0 copy-done
  7.6 0.0 copy-start.4
  7.6 2.4 pad_maximum_fusion
  10.0 0.0 all-gather.8.cloned.1.call-update
  10.0 0.0 all-gather.6.cloned.1.call-start
  10.1 1.3 fusion.3
  11.4 0.0 copy-done.2
  11.4 1.7 fusion.5
  13.1 0.0 copy-start.5
  13.1 0.0 all-gather.6.cloned.1.call-update
  13.1 0.0 all-gather.10.cloned.1.call-start
  13.2 0.9 constant_dynamic-slice_fusion.1
  14.1 0.0 copy-done.3
  14.1 1.1 pad_maximum_fusion.1
  15.2 0.0 all-gather.10.cloned.1.call-update
  15.2 0.0 all-gather.12.cloned.1.call-start
  15.2 0.9 constant_dynamic-slice_fusion
  16.1 0.0 copy-done.4
  16.1 1.1 pad_maximum_fusion.2
  17.2 0.0 all-gather.12.cloned.1.call-update
  17.2 0.0 copy-start.8
  17.2 0.0 copy-start.6
  17.2 0.0 copy-start.7
  17.2 0.0 copy-start.1
  17.2 1.3 copy.40
  18.5 0.0 copy-done.5
  18.6 0.2 copy.41
  18.8 0.1 maximum_bitcast_fusion
  18.9 1.2 copy.42
  20.0 7.3 %all-to-all-start = ((bf16[8,2,256,128]{2,3,1,0:T(8,128)(2,1)}), bf16[8,2,256,128]{2,3,1,0:T(8,128)(2,1)S(1)}, u32[]{:S(2)}, u32[]{:S(2)}) async-start(bf16[8,2,256,128]{2,3,1,0:T(8,128)(2,1)} %copy.42), calls=%async_computation | async-start | bytes 2097152 | tf_op jit(solution)/shard_map/all_to_all | solution.py:58
  27.4 0.0 reduce-scatter.2.cloned.1.call-start
  27.4 0.0 copy-done.8
  27.4 0.0 copy-done.6
  27.4 0.0 copy-done.7
  27.5 0.0 copy-done.1
  27.5 0.3 fusion.19
  27.8 46.5 %all-gather = f32[8,144,17]{1,2,0:T(8,128)S(1)} all-gather(f32[1,144,17]{1,2,0:T(8,128)S(1)} %maximum_bitcast_fusion.1), channel_id=1, replica_groups=mesh['ep'=8,'tp'=4] {'ep'}, dimensions={0}, use_global_device_ids=true | all-gather | bytes 88128 | tf_op jit(solution)/shard_map/all_gather | solution.py:46
  74.3 0.1 reshape.59
  74.5 0.0 all-to-all-done
  74.6 0.1 fusion.15
  74.6 0.3 copy.46
  74.9 0.3 copy.45
  75.2 0.0 all-gather.8.cloned.1.call-done
  75.2 55.7 %all-gather.6.cloned.1.call-done = bf16[1152,2048]{1,0:T(8,128)(2,1)} async-done(((bf16[144,2048]{1,0:T(8,128)(2,1)}), bf16[1152,2048]{1,0:T(8,128)(2,1)}) %all-gather.6.cloned.1.call-update) | async-done | bytes 4718608 | tf_op jit(solution)/shard_map/all_gather | solution.py:45
  130.9 10.7 %fusion.18 = f32[1152,1088]{0,1:T(8,128)} fusion(bf16[1152,2048]{1,0:T(8,128)(2,1)} %all-gather.6.cloned.1.call-done, bf16[1088,2048]{1,0:T(8,128)(2,1)} %all-gather.8.cloned.1.call-done), kind=kOutput, calls=%fused_computation.46 | convolution fusion | flops 5133828096 | bytes 14188544 | tf_op jit(solution)/shard_map/td,fd->tf/dot_general | solution.py:69
  141.6 25.2 %all-gather.10.cloned.1.call-done = bf16[1088,2048]{1,0:T(8,128)(2,1)} async-done(((bf16[272,2048]{1,0:T(8,128)(2,1)}), bf16[1088,2048]{1,0:T(8,128)(2,1)}) %all-gather.10.cloned.1.call-update) | async-done | bytes 4456464 | tf_op jit(solution)/shard_map/all_gather | solution.py:53
  166.8 37.4 %all-gather.12.cloned.1.call-done = bf16[1088,2048]{1,0:T(8,128)(2,1)} async-done(((bf16[272,2048]{1,0:T(8,128)(2,1)}), bf16[1088,2048]{1,0:T(8,128)(2,1)}) %all-gather.12.cloned.1.call-update) | async-done | bytes 4456464 | tf_op jit(solution)/shard_map/all_gather | solution.py:54
  204.2 25.3 %fusion.20 = f32[1152,2048]{1,0:T(8,128)} fusion(bf16[1088,2048]{1,0:T(8,128)(2,1)} %all-gather.12.cloned.1.call-done, bf16[1152,2048]{1,0:T(8,128)(2,1)} %all-gather.6.cloned.1.call-done, bf16[1088,2048]{1,0:T(8,128)(2,1)} %all-gather.10.cloned.1.call-done, f32[1152,1088]{0,1:T(8,128)} %fusion.18, f32[1152]{0:T(1024)S(1)} %get-tuple-element.7, ...), kind=kOutput, calls=%fused_computation.48 | convolution fusion | flops 10278936576 | bytes 28093568 | tf_op jit(solution)/shard_map/dot_general | solution.py:74
  229.5 11.4 %fusion.1 = bf16[1152,2048]{1,0:T(8,128)(2,1)} fusion(f32[1152,2048]{1,0:T(8,128)} %fusion.20, bf16[2048,128]{1,0:T(8,128)(2,1)S(1)} %bitcast.34, f32[1152]{0:T(1024)S(1)} %get-tuple-element.5, bf16[1152,2048]{1,0:T(8,128)(2,1)} %all-gather.6.cloned.1.call-done, bf16[2048,128]{1,0:T(8,128)(2,1)S(1)} %bitcast.35), kind=kOutput, calls=%fused_computation.3 | convolution fusion | flops 1213562880 | bytes 19927552 | tf_op jit(solution)/shard_map/ts,ds->td/dot_general | solution.py:75
  240.9 0.0 reduce-scatter.2.cloned.1.call-update
  240.9 95.8 %reduce-scatter.2.cloned.1.call-done = bf16[144,2048]{1,0:T(8,128)(2,1)} async-done(((bf16[1152,2048]{1,0:T(8,128)(2,1)}), bf16[144,2048]{1,0:T(8,128)(2,1)}) %reduce-scatter.2.cloned.1.call-update) | async-done | bytes 589840 | tf_op jit(solution)/shard_map/reduce_scatter | solution.py:76
  (9 shorter events, 0.2 us)
Async XLA Ops:
  6.5 1.0 copy-start
  6.5 4.8 %copy-start.2 = (bf16[144,2048]{1,0:T(8,128)(2,1)S(1)}, bf16[144,2048]{1,0:T(8,128)(2,1)}, u32[]{:S(2)}) copy-start(bf16[144,2048]{1,0:T(8,128)(2,1)} %param.13) | copy-start | bytes 1769476
  6.5 7.5 %copy-start.3 = (bf16[2,128,2048]{2,1,0:T(8,128)(2,1)S(1)}, bf16[2,128,2048]{2,1,0:T(8,128)(2,1)}, u32[]{:S(2)}) copy-start(bf16[2,128,2048]{2,1,0:T(8,128)(2,1)} %param.18) | copy-start | bytes 3145732
  6.5 68.7 %all-gather.8.cloned.1.call-start = ((), (), s32[]{:S(2)}) async-start(), calls=%async_computation.3 | async-start | bytes 5570560 | tf_op jit(solution)/shard_map/all_gather | solution.py:52
  7.6 8.5 %copy-start.4 = (bf16[2,128,2048]{2,1,0:T(8,128)(2,1)S(1)}, bf16[2,128,2048]{2,1,0:T(8,128)(2,1)}, u32[]{:S(2)}) copy-start(bf16[2,128,2048]{2,1,0:T(8,128)(2,1)} %param.19) | copy-start | bytes 3145732
  10.0 120.9 %all-gather.6.cloned.1.call-start = ((), (), s32[]{:S(2)}) async-start(), calls=%async_computation.2 | async-start | bytes 5308416 | tf_op jit(solution)/shard_map/all_gather | solution.py:45
  13.1 5.5 %copy-start.5 = (bf16[256,1024]{1,0:T(8,128)(2,1)S(1)}, bf16[256,1024]{1,0:T(8,128)(2,1)}, u32[]{:S(2)}) copy-start(bf16[256,1024]{1,0:T(8,128)(2,1)} %param.24) | copy-start | bytes 1572868
  13.1 153.7 %all-gather.10.cloned.1.call-start = ((), (), s32[]{:S(2)}) async-start(), calls=%async_computation.4 | async-start | bytes 5570560 | tf_op jit(solution)/shard_map/all_gather | solution.py:53
  15.2 189.0 %all-gather.12.cloned.1.call-start = ((), (), s32[]{:S(2)}) async-start(), calls=%async_computation.5 | async-start | bytes 5570560 | tf_op jit(solution)/shard_map/all_gather | solution.py:54
  17.2 10.2 %copy-start.8 = (bf16[2048]{0:T(1024)(128)(2,1)S(1)}, bf16[2048]{0:T(1024)(128)(2,1)}, u32[]{:S(2)}) copy-start(bf16[2048]{0:T(1024)(128)(2,1)} %param.25) | copy-start | bytes 12292
  17.2 10.2 %copy-start.6 = (f32[144,8]{0,1:T(8,128)S(1)}, f32[144,8]{0,1:T(8,128)}, u32[]{:S(2)}) copy-start(f32[144,8]{0,1:T(8,128)} %param.16) | copy-start | bytes 13828
  17.2 10.2 %copy-start.7 = (s32[144,8]{0,1:T(8,128)S(1)}, s32[144,8]{0,1:T(8,128)}, u32[]{:S(2)}) copy-start(s32[144,8]{0,1:T(8,128)} %param.15) | copy-start | bytes 13828
  17.2 10.3 %copy-start.1 = (bf16[144,2048]{1,0:T(8,128)(2,1)S(1)}, bf16[144,2048]{1,0:T(8,128)(2,1)}, u32[]{:S(2)}) copy-start(bf16[144,2048]{1,0:T(8,128)(2,1)} %fusion.5) | copy-start | bytes 1769476
  20.0 54.5 %all-to-all-start = ((bf16[8,2,256,128]{2,3,1,0:T(8,128)(2,1)}), bf16[8,2,256,128]{2,3,1,0:T(8,128)(2,1)S(1)}, u32[]{:S(2)}, u32[]{:S(2)}) async-start(bf16[8,2,256,128]{2,3,1,0:T(8,128)(2,1)} %copy.42), calls=%async_computation | async-start | bytes 2097152 | tf_op jit(solution)/shard_map/all_to_all | solution.py:58
  27.4 309.4 %reduce-scatter.2.cloned.1.call-start = ((), (), s32[]{:S(2)}) async-start(), calls=%async_computation.6 | async-start | bytes 5308416 | tf_op jit(solution)/shard_map/reduce_scatter | solution.py:76
Sparse Core Ops, SparseCore 0:
  10.2 38.6 all-gather.7
  51.1 79.8 all-gather.5
  132.5 34.3 all-gather.9
  168.3 35.9 all-gather.11
  241.0 95.6 reduce-scatter.1

commit v2 on v1

v2 whole, which is shorter than its diff:
```python
import functools

import jax
import jax.numpy as jnp
from jax import lax
from jax.experimental import pallas as pl
from jax.experimental.pallas import tpu as pltpu
from jax.sharding import PartitionSpec as P

norm_eps = 1.0
MESH = pl.DeviceIdType.MESH
NT = (((1,), (1,)), ((), ()))


def normalize(tokens, norm_gain):
    values = tokens.astype(jnp.float32)
    scale_inv = lax.rsqrt(jnp.mean(values * values, axis=-1, keepdims=True) + norm_eps)
    return (values * scale_inv * norm_gain).astype(jnp.bfloat16)


def silu(v):
    return v / (1.0 + jnp.exp(-v))


def kernel(
    dims,
    payload_ref, gate_ref, up_ref, down_ref, side_ref, mask_ref,
    out_ref,
    tok, wg, wu, wd, side, hidden, side_hid, acc, xs, xr, sent, got,
    tok_send, tok_recv, w_send, w_recv, side_send, side_recv,
    x_send, x_recv, r_send, r_recv, l_send, l_recv,
):
    nz, nx, ny, nc, experts_all, local_experts, chunks = dims
    n_ep, n_tp = nz * nx, ny * nc
    me, tp = lax.axis_index("ep"), lax.axis_index("tp")
    z, x = me // nx, me % nx
    y, c = tp // nc, tp % nc
    rows = payload_ref.shape[0]
    width = out_ref.shape[1]
    part = gate_ref.shape[0]
    piece = width // chunks
    side_rows = side_ref.shape[2]

    def cols(q):
        return pl.ds(pl.multiple_of(q * piece, piece), piece)

    barrier = pltpu.get_barrier_semaphore()
    for j in range(1, n_ep):
        pl.semaphore_signal(barrier, inc=1, device_id=((me + j) % n_ep, tp), device_id_type=MESH)
    for j in range(1, n_tp):
        pl.semaphore_signal(barrier, inc=1, device_id=(me, (tp + j) % n_tp), device_id_type=MESH)
    pl.semaphore_wait(barrier, n_ep + n_tp - 2)

    def tok_rows(bz, bx):
        return pl.ds(pl.multiple_of((bx * nz + bz) * rows, rows), rows)

    def tok_copy(bz, way, own):
        if way < 2:
            target = (me + nx if way == 0 else me - nx, tp)
        else:
            target = (z * nx + (x + way - 1) % nx, tp)
        return pltpu.make_async_remote_copy(
            src_ref=payload_ref if own else tok.at[tok_rows(bz, x)],
            dst_ref=tok.at[tok_rows(bz, x)],
            send_sem=tok_send.at[bz, way],
            recv_sem=tok_recv.at[x * nz + bz],
            device_id=target,
            device_id_type=MESH,
        )

    def tok_wait(bz, bx):
        pltpu.make_async_remote_copy(
            src_ref=payload_ref,
            dst_ref=tok.at[tok_rows(bz, bx)],
            send_sem=tok_send.at[0, 0],
            recv_sem=tok_recv.at[bx * nz + bz],
            device_id=(me, tp),
            device_id_type=MESH,
        ).wait_recv()

    def w_refs(k, owner, own):
        if k == 0:
            return (gate_ref if own else wg.at[owner]), wg.at[owner]
        if k == 1:
            return (up_ref if own else wu.at[owner]), wu.at[owner]
        q = cols(k - 2)
        return (down_ref.at[:, q] if own else wd.at[owner, :, q]), wd.at[owner, :, q]

    def w_copy(k, by, way, own):
        if way < 2:
            target = (me, tp + nc if way == 0 else tp - nc)
        else:
            target = (me, y * nc + (c + way - 1) % nc)
        owner = by * nc + c
        src, dst = w_refs(k, owner, own)
        return pltpu.make_async_remote_copy(
            src_ref=src,
            dst_ref=dst,
            send_sem=w_send.at[k, by, way],
            recv_sem=w_recv.at[k, owner],
            device_id=target,
            device_id_type=MESH,
        )

    def w_wait(k, owner):
        src, dst = w_refs(k, owner, True)
        pltpu.make_async_remote_copy(
            src_ref=src, dst_ref=dst, send_sem=w_send.at[0, 0, 0], recv_sem=w_recv.at[k, owner],
            device_id=(me, tp), device_id_type=MESH,
        ).wait_recv()

    def side_copy(j):
        to = (me + j) % n_ep
        return pltpu.make_async_remote_copy(
            src_ref=side_ref.at[to],
            dst_ref=side.at[me],
            send_sem=side_send.at[j],
            recv_sem=side_recv.at[me],
            device_id=(to, tp),
            device_id_type=MESH,
        )

    def each_own(copy_of, at, last, ways, act):
        @pl.when(at < last)
        def _():
            act(copy_of(0))

        @pl.when(at > 0)
        def _():
            act(copy_of(1))

        for way in range(2, ways):
            act(copy_of(way))

    def each_forward(copy_of, index_of, at, last, ways, step, act, arrive):
        @pl.when(at >= step)
        def _():
            b = at - step
            arrive(b)

            @pl.when(at < last)
            def _():
                act(copy_of(b, 0))

            for way in range(2, ways):
                act(copy_of(b, way))

        @pl.when(at + step <= last)
        def _():
            b = at + step
            arrive(b)

            @pl.when(at > 0)
            def _():
                act(copy_of(b, 1))

            for way in range(2, ways):
                act(copy_of(b, way))

    start = lambda copy: copy.start()
    finish = lambda copy: copy.wait_send()
    nothing = lambda b: None
    tok_ways, w_ways = 1 + nx, 1 + nc
    pieces = 2 + chunks

    def tok_forward(step, act, arrive):
        each_forward(
            lambda b, way: tok_copy(b, way, False), None, z, nz - 1, tok_ways, step, act, arrive
        )

    def w_forward(k, step, act, arrive):
        each_forward(
            lambda b, way: w_copy(k, b, way, False), None, y, ny - 1, w_ways, step, act, arrive
        )

    def w_gathered(k):
        for step in range(1, ny):
            w_forward(k, step, start, lambda b: w_wait(k, b * nc + c))

    def w_across(k):
        for j in range(1, nc):
            for by in range(ny):
                w_wait(k, by * nc + (c + j) % nc)

    each_own(lambda way: tok_copy(z, way, True), z, nz - 1, tok_ways, start)
    for k in range(pieces):
        each_own(lambda way: w_copy(k, y, way, True), y, ny - 1, w_ways, start)
    for j in range(1, n_ep):
        side_copy(j).start()
    tok[tok_rows(z, x)] = payload_ref[...]
    wg[tp] = gate_ref[...]
    wu[tp] = up_ref[...]
    wd[tp] = down_ref[...]
    side[me] = side_ref[me]

    def arrive_tok(b):
        tok_wait(b, x)

    for step in range(1, nz):
        tok_forward(step, start, arrive_tok)
        if step == nz - 2:
            w_gathered(0)
    w_gathered(1)
    w_across(0)
    w_across(1)
    for j in range(1, n_ep):
        b = (me + j) % n_ep
        pltpu.make_async_remote_copy(
            src_ref=side_ref.at[b], dst_ref=side.at[b], send_sem=side_send.at[0],
            recv_sem=side_recv.at[b], device_id=(me, tp), device_id_type=MESH,
        ).wait_recv()

    tile = 2 * rows
    for j in range(nx):
        bx = (x + j) % nx
        if j:
            for bz in range(nz):
                tok_wait(bz, bx)

        def hidden_tile(i, carry):
            at = pl.ds(pl.multiple_of(bx * nz * rows + i * tile, rows), tile)
            a = tok[at, :width]
            gate_part = lax.dot_general(
                a, wg[...].reshape(n_tp * part, width), NT, preferred_element_type=jnp.float32
            )
            up_part = lax.dot_general(
                a, wu[...].reshape(n_tp * part, width), NT, preferred_element_type=jnp.float32
            )
            aux = tok[at, width:].astype(jnp.float32)
            lane = lax.broadcasted_iota(jnp.int32, aux.shape, 1)

            def column(n):
                hit = jnp.logical_or(lane == n, lane == n + 64)
                return jnp.sum(jnp.where(hit, aux, 0.0), axis=1, keepdims=True)

            scale = mask_ref[local_experts : local_experts + 1, :]
            for e in range(local_experts):
                scale = scale + column(me * local_experts + e) * mask_ref[e : e + 1, :]
            hidden[at] = (silu(gate_part) * up_part * scale).astype(jnp.bfloat16)
            side_part = jnp.dot(
                a, side[:, 0].reshape(width, side.shape[3]), preferred_element_type=jnp.float32
            )
            side_hid[at] = (silu(side_part) * column(experts_all)).astype(jnp.bfloat16)
            return carry

        lax.fori_loop(0, nz * rows // tile, hidden_tile, 0)

    def x_copy(q, j, bz):
        block = pl.ds(bz * rows, rows)
        return pltpu.make_async_remote_copy(
            src_ref=xs.at[q, j - 1, block],
            dst_ref=xr.at[q, j - 1, block],
            send_sem=x_send.at[q, j - 1, bz],
            recv_sem=x_recv.at[q, j - 1, bz],
            device_id=(z * nx + (x + j) % nx, tp),
            device_id_type=MESH,
        )

    def r_copy(q, dz):
        return pltpu.make_async_remote_copy(
            src_ref=sent.at[q, dz], dst_ref=got.at[q, dz + 1], send_sem=r_send.at[q, dz],
            recv_sem=r_recv.at[q, dz], device_id=(me + nx, tp), device_id_type=MESH,
        )

    def l_copy(q, dz):
        return pltpu.make_async_remote_copy(
            src_ref=sent.at[q, dz], dst_ref=got.at[q, dz], send_sem=l_send.at[q, dz],
            recv_sem=l_recv.at[q, dz], device_id=(me - nx, tp), device_id_type=MESH,
        )

    blocks_per = piece // side_rows

    def multiply(q):
        down = wd[:, :, cols(q)].reshape(n_tp * part, piece)
        side_down = side[pl.ds(q * blocks_per, blocks_per), 1].reshape(piece, side.shape[3])
        for j in list(range(1, nx)) + [0]:
            at = pl.ds(pl.multiple_of((x + j) % nx * nz * rows, rows), nz * rows)
            value = jnp.dot(hidden[at], down, preferred_element_type=jnp.float32)
            value = value + lax.dot_general(
                side_hid[at], side_down, NT, preferred_element_type=jnp.float32
            )
            if j:
                xs[q, j - 1] = value.astype(jnp.bfloat16)
                for bz in range(nz):
                    x_copy(q, j, bz).start()
            else:
                acc[q] = value

    def reduce(q):
        def own(dz):
            block = pl.ds(pl.multiple_of(dz * rows, rows), rows)
            value = acc[q, block]
            for j in range(1, nx):
                x_copy(q, j, dz).wait_recv()
                value = value + xr[q, j - 1, block].astype(jnp.float32)
            return value

        def right(dz):
            value = own(dz)

            @pl.when(z == 0)
            def _():
                sent[q, dz] = value.astype(jnp.bfloat16)

            @pl.when(z > 0)
            def _():
                r_copy(q, dz).wait_recv()
                sent[q, dz] = (value + got[q, dz + 1].astype(jnp.float32)).astype(jnp.bfloat16)

            r_copy(q, dz).start()

        def left(dz):
            value = own(dz)

            @pl.when(z == nz - 1)
            def _():
                sent[q, dz] = value.astype(jnp.bfloat16)

            @pl.when(z < nz - 1)
            def _():
                l_copy(q, dz).wait_recv()
                sent[q, dz] = (value + got[q, dz].astype(jnp.float32)).astype(jnp.bfloat16)

            l_copy(q, dz).start()

        for k in range(nz - 1):
            pl.when(z < nz - 1 - k)(functools.partial(right, nz - 1 - k))
            pl.when(z > k)(functools.partial(left, k))
        acc[q, pl.ds(0, rows)] = own(z)

    def settle(q):
        @pl.when(z > 0)
        def _():
            r_copy(q, z).wait_recv()
            acc[q, pl.ds(0, rows)] += got[q, z + 1].astype(jnp.float32)

        @pl.when(z < nz - 1)
        def _():
            l_copy(q, z).wait_recv()
            acc[q, pl.ds(0, rows)] += got[q, z].astype(jnp.float32)

        out_ref[:, cols(q)] = acc[q, pl.ds(0, rows)].astype(jnp.bfloat16)

    for q in range(chunks):
        w_gathered(2 + q)
        w_across(2 + q)
        multiply(q)
        if q:
            reduce(q - 1)
    reduce(chunks - 1)
    for q in range(chunks):
        settle(q)

    each_own(lambda way: tok_copy(z, way, True), z, nz - 1, tok_ways, finish)
    for step in range(1, nz):
        tok_forward(step, finish, nothing)
    for k in range(pieces):
        each_own(lambda way: w_copy(k, y, way, True), y, ny - 1, w_ways, finish)
        for step in range(1, ny):
            w_forward(k, step, finish, nothing)
    for j in range(1, n_ep):
        side_copy(j).wait_send()
    for q in range(chunks):
        for j in range(1, nx):
            for bz in range(nz):
                x_copy(q, j, bz).wait_send()
        for dz in range(nz):
            pl.when(z < dz)(lambda: r_copy(q, dz).wait_send())
            pl.when(z > dz)(lambda: l_copy(q, dz).wait_send())


def body(
    nx,
    nc,
    tokens,
    norm_gain,
    expert_ids,
    route_weights,
    expert_gate,
    expert_up,
    expert_down,
    shared_gate,
    shared_up,
    shared_down,
    side_in,
    side_out,
    side_gate,
):
    normed = normalize(tokens, norm_gain)
    tok_count, width = normed.shape
    n_ep, n_tp = lax.axis_size("ep"), lax.axis_size("tp")
    nz, ny = n_ep // nx, n_tp // nc
    me = lax.axis_index("ep")
    local_experts, ff_part, _ = expert_gate.shape
    experts_all = n_ep * local_experts
    shared_rows = shared_gate.shape[0] // n_ep
    side_rows, side_all = side_in.shape
    side_cols = side_all // n_ep
    chunks = 4
    piece = width // chunks

    named = expert_ids[:, :, None] == jnp.arange(experts_all, dtype=jnp.int32)
    dense = jnp.sum(jnp.where(named, route_weights[:, :, None], 0.0), axis=1)
    opening = jax.nn.sigmoid(jnp.dot(normed, side_gate, preferred_element_type=jnp.float32))
    aux = jnp.concatenate([dense, opening[:, None]], axis=1)
    aux = jnp.pad(aux, ((0, 0), (0, 64 - aux.shape[1])))
    high = lax.reduce_precision(aux, 8, 7)
    payload = jnp.concatenate(
        [normed, high.astype(jnp.bfloat16), (aux - high).astype(jnp.bfloat16)], axis=1
    )

    used = local_experts * ff_part + shared_rows
    part = -(-used // 16) * 16

    def pack(expert_part, shared_part):
        own = lax.dynamic_slice_in_dim(shared_part, me * shared_rows, shared_rows, 0)
        own = jnp.pad(own, ((0, part - used), (0, 0)))
        return jnp.concatenate([expert_part.reshape(local_experts * ff_part, width), own], axis=0)

    both = jnp.stack([side_in, side_out]).reshape(2, side_rows, n_ep, side_cols)
    both = both.transpose(2, 0, 1, 3)
    place = jnp.arange(n_tp * part, dtype=jnp.int32) % part // ff_part
    place = jnp.minimum(place, local_experts)
    mask = (place[None, :] == jnp.arange(local_experts + 1)[:, None]).astype(jnp.float32)

    bf16, f32 = jnp.bfloat16, jnp.float32
    dma = pltpu.SemaphoreType.DMA
    dims = (nz, nx, ny, nc, experts_all, local_experts, chunks)
    return pl.pallas_call(
        functools.partial(kernel, dims),
        out_shape=jax.ShapeDtypeStruct((tok_count, width), bf16),
        in_specs=[pl.BlockSpec(memory_space=pltpu.VMEM)] * 6,
        out_specs=pl.BlockSpec(memory_space=pltpu.VMEM),
        scratch_shapes=[
            pltpu.VMEM((n_ep * tok_count, payload.shape[1]), bf16),
            pltpu.VMEM((n_tp, part, width), bf16),
            pltpu.VMEM((n_tp, part, width), bf16),
            pltpu.VMEM((n_tp, part, width), bf16),
            pltpu.VMEM((n_ep, 2, side_rows, side_cols), bf16),
            pltpu.VMEM((n_ep * tok_count, n_tp * part), bf16),
            pltpu.VMEM((n_ep * tok_count, side_cols), bf16),
            pltpu.VMEM((chunks, nz * tok_count, piece), f32),
            pltpu.VMEM((chunks, nx - 1, nz * tok_count, piece), bf16),
            pltpu.VMEM((chunks, nx - 1, nz * tok_count, piece), bf16),
            pltpu.VMEM((chunks, nz, tok_count, piece), bf16),
            pltpu.VMEM((chunks, nz + 1, tok_count, piece), bf16),
            dma((nz, 1 + nx)),
            dma((n_ep,)),
            dma((2 + chunks, ny, 1 + nc)),
            dma((2 + chunks, n_tp)),
            dma((n_ep,)),
            dma((n_ep,)),
            dma((chunks, nx - 1, nz)),
            dma((chunks, nx - 1, nz)),
            dma((chunks, nz)),
            dma((chunks, nz)),
            dma((chunks, nz)),
            dma((chunks, nz)),
        ],
        compiler_params=pltpu.CompilerParams(
            collective_id=0, has_side_effects=True, vmem_limit_bytes=63000 * 1024
        ),
        name="layer",
    )(payload, pack(expert_gate, shared_gate), pack(expert_up, shared_up),
      pack(expert_down, shared_down), both, mask)


def solution(mesh):
    devices = mesh.devices
    nx = len({d.coords[0] for d in devices[:, 0]})
    nc = len({d.core_on_chip for d in devices[0, :]})
    placed = (
        P(("ep", "tp"), None),
        P(),
        P(("ep", "tp"), None),
        P(("ep", "tp"), None),
        P("ep", "tp", None),
        P("ep", "tp", None),
        P("ep", "tp", None),
        P("tp", None),
        P("tp", None),
        P("tp", None),
        P("ep", None),
        P("ep", None),
        P(),
    )
    return jax.shard_map(
        functools.partial(body, nx, nc),
        mesh=mesh,
        in_specs=placed,
        out_specs=P(("ep", "tp"), None),
        check_vma=False,
    )
```

time: 344 us -> 190 us (0.55)
  waiting for transfers between devices: 214 us -> 0 us
  Pallas kernels: 0 us -> 175 us
  matrix products: 47.6 us -> 0.25 us
  blocking collectives: 46.5 us -> 0 us
  between operations: 13.3 us -> 0.13 us
  starting transfers between devices: 7.49 us -> 0 us
    pallas_call x0 -> x1, Pallas kernels: none -> 175 us  [body(): pl.pallas_call(functools.partial(kernel, dims), out_shape=jax.ShapeDtypeS...]
    all_gather x4 -> x0, waiting for transfers between devices: 118 us -> none  [the longest x1 55.7 us: body(): all_normed = lax.all_gather(normed, 'ep', axis=0, tiled=True)]
    reduce_scatter x1 -> x0, waiting for transfers between devices: 95.8 us -> none  [body(): lax.psum_scatter(total.astype(jnp.bfloat16), 'ep', scatter_dimension=0, t...]
    dot_general x3 -> x0, matrix products: 47.3 us -> none  [the longest x1 25.3 us: body(): total = jnp.dot(hidden, down_all, preferred_element_type=jnp.float32)]
    all_gather x1 -> x0, blocking collectives: 46.5 us -> none  [body(): all_aux = lax.all_gather(aux, 'ep', axis=0, tiled=True)]
    all_to_all x1 -> x0, starting transfers between devices: 7.33 us -> none  [body(): lax.all_to_all(both.transpose(2, 0, 1, 3), 'ep', split_axis=0, concat_axi...]
  transfers between devices with their start and end apart: 6 -> 0, of which waited for: 4 -> 0; matrix products, arithmetic and copies ran while one was open for 6% -> 0% of each run, Pallas kernels for 0% -> 0%
where the time goes in v2:
time: 190 us
  Pallas kernels  175 us (92%)
  local copies, waits for them, and re-layouts  7.33 us (4%)
  other arithmetic  7.32 us (4%)
    pallas_call x1, Pallas kernels, body(): pl.pallas_call(functools.partial(kernel, dims), out_shape=jax.ShapeDtypeS...  175 us
    unnamed x20, local copies, waits for them, and re-layouts  4.78 us

profile of v2, /device:TPU:0, one launch (start us, length us, event | category | flops | bytes accessed | tf_op | source)
XLA Modules:
  0.0 189.7 jit_solution(4415035329743109113)
XLA Ops:
  0.0 0.0 copy-start
  0.0 0.0 copy-start.5
  0.0 1.4 fusion
  1.4 0.7 reshape.53
  2.1 0.6 fusion.4.mask_ref
  2.7 0.7 select_reduce_fusion
  3.4 0.0 copy-done
  3.5 0.9 constant_dynamic-slice_fusion
  4.4 0.0 copy-start.6
  4.4 0.0 copy-done.5
  4.4 0.2 copy.31
  4.6 0.3 copy.33
  4.9 0.5 copy-done.6
  5.4 0.2 copy.32
  5.6 0.3 copy.34
  5.9 0.0 copy-start.1
  5.9 0.0 copy-start.7
  5.9 1.1 maximum_bitcast_fusion.side_ref
  7.0 0.1 copy-done.1
  7.1 0.0 copy-done.7
  7.1 0.2 fusion.2
  7.3 0.0 copy-start.2
  7.3 0.3 fusion.12
  7.6 0.1 copy.30
  7.7 1.0 concatenate.17.payload_ref
  8.7 0.0 copy-done.2
  8.7 0.0 copy-start.3
  8.7 1.1 pad_maximum_fusion.2.down_ref
  9.8 0.6 copy-done.3
  10.4 0.0 copy-start.4
  10.4 1.1 pad_maximum_fusion.gate_ref
  11.4 0.6 copy-done.4
  12.0 1.1 pad_maximum_fusion.1.up_ref
  13.1 174.7 %layer.1 = bf16[144,2048]{1,0:T(8,128)(2,1)} custom-call(bf16[144,2176]{1,0:T(8,128)(2,1)} %concatenate.17.payload_ref, bf16[272,2048]{1,0:T(8,128)(2,1)} %pad_maximum_fusion.gate_ref, bf16[272,2048]{1,0:T(8,128)(2,1)} %pad_maximum_fusion.1.up_ref, bf16[272,2048]{1,0:T(8,128)(2,1)} %pad_maximum_fusion.2.down_ref, ...), custom_call_target="tpu_custom_call" | custom-call | tf_op jit(solution)/shard_map/layer/pallas_call | solution.py:429
  187.8 1.9 %copy.36 = bf16[144,2048]{1,0:T(8,128)(2,1)} copy(bf16[144,2048]{1,0:T(8,128)(2,1)} %layer.1) | data formatting | bytes 1179648
  (6 shorter events, 0.1 us)
Async XLA Ops:
  0.0 3.4 %copy-start = (bf16[128,2048]{1,0:T(8,128)(2,1)S(1)}, bf16[128,2048]{1,0:T(8,128)(2,1)}, u32[]{:S(2)}) copy-start(bf16[128,2048]{1,0:T(8,128)(2,1)} %param.20) | copy-start | bytes 1572868
  0.0 4.4 %copy-start.5 = (bf16[256,1024]{1,0:T(8,128)(2,1)S(1)}, bf16[256,1024]{1,0:T(8,128)(2,1)}, u32[]{:S(2)}) copy-start(bf16[256,1024]{1,0:T(8,128)(2,1)} %param.23) | copy-start | bytes 1572868
  4.4 1.0 copy-start.6
  5.9 1.2 copy-start.1
  5.9 1.2 copy-start.7
  7.3 1.4 copy-start.2
  8.7 1.6 copy-start.3
  10.4 1.6 copy-start.4

commit v3 on v2

--- a/solution.py
+++ b/solution.py
@@ -2,6 +2,7 @@
 
 import jax
 import jax.numpy as jnp
+import numpy as np
 from jax import lax
 from jax.experimental import pallas as pl
 from jax.experimental.pallas import tpu as pltpu
@@ -12,22 +13,17 @@
 NT = (((1,), (1,)), ((), ()))
 
 
-def normalize(tokens, norm_gain):
-    values = tokens.astype(jnp.float32)
-    scale_inv = lax.rsqrt(jnp.mean(values * values, axis=-1, keepdims=True) + norm_eps)
-    return (values * scale_inv * norm_gain).astype(jnp.bfloat16)
-
-
 def silu(v):
     return v / (1.0 + jnp.exp(-v))
 
 
 def kernel(
     dims,
-    payload_ref, gate_ref, up_ref, down_ref, side_ref, mask_ref,
+    tokens_ref, gain_ref, ids_ref, route_ref, side_gate_ref, mask_ref,
+    gate_ref, up_ref, down_ref, s_gate_ref, s_up_ref, s_down_ref, side_in_ref, side_out_ref,
     out_ref,
     tok, wg, wu, wd, side, hidden, side_hid, acc, xs, xr, sent, got,
-    tok_send, tok_recv, w_send, w_recv, side_send, side_recv,
+    tok_send, tok_recv, w_send, w_recv, side_send, side_recv, swap_send, swap_recv, local_sem,
     x_send, x_recv, r_send, r_recv, l_send, l_recv,
 ):
     nz, nx, ny, nc, experts_all, local_experts, chunks = dims
@@ -35,11 +31,13 @@
     me, tp = lax.axis_index("ep"), lax.axis_index("tp")
     z, x = me // nx, me % nx
     y, c = tp // nc, tp % nc
-    rows = payload_ref.shape[0]
+    rows = tokens_ref.shape[0]
     width = out_ref.shape[1]
-    part = gate_ref.shape[0]
+    routed = gate_ref.shape[0]
+    part, side_cols = wg.shape[1], side.shape[2]
+    extra = part - routed
     piece = width // chunks
-    side_rows = side_ref.shape[2]
+    side_rows = side.shape[1]
 
     def cols(q):
         return pl.ds(pl.multiple_of(q * piece, piece), piece)
@@ -54,13 +52,13 @@
     def tok_rows(bz, bx):
         return pl.ds(pl.multiple_of((bx * nz + bz) * rows, rows), rows)
 
-    def tok_copy(bz, way, own):
+    def tok_copy(bz, way):
         if way < 2:
             target = (me + nx if way == 0 else me - nx, tp)
         else:
             target = (z * nx + (x + way - 1) % nx, tp)
         return pltpu.make_async_remote_copy(
-            src_ref=payload_ref if own else tok.at[tok_rows(bz, x)],
+            src_ref=tok.at[tok_rows(bz, x)],
             dst_ref=tok.at[tok_rows(bz, x)],
             send_sem=tok_send.at[bz, way],
             recv_sem=tok_recv.at[x * nz + bz],
@@ -70,7 +68,7 @@
 
     def tok_wait(bz, bx):
         pltpu.make_async_remote_copy(
-            src_ref=payload_ref,
+            src_ref=tok.at[tok_rows(bz, bx)],
             dst_ref=tok.at[tok_rows(bz, bx)],
             send_sem=tok_send.at[0, 0],
             recv_sem=tok_recv.at[bx * nz + bz],
@@ -78,21 +76,35 @@
             device_id_type=MESH,
         ).wait_recv()
 
-    def w_refs(k, owner, own):
+    def w_place(k, owner):
         if k == 0:
-            return (gate_ref if own else wg.at[owner]), wg.at[owner]
+            return wg.at[owner]
         if k == 1:
-            return (up_ref if own else wu.at[owner]), wu.at[owner]
-        q = cols(k - 2)
-        return (down_ref.at[:, q] if own else wd.at[owner, :, q]), wd.at[owner, :, q]
-
-    def w_copy(k, by, way, own):
+            return wu.at[owner]
+        return wd.at[owner, :, cols(k - 2)]
+
+    def own_parts(ref, shared_ref, place, q=None):
+        at = pl.ds(pl.multiple_of(me * extra, extra), extra)
+        at = at if shared_ref.shape[0] > extra else pl.ds(0, extra)
+        head, tail = pl.ds(0, routed), pl.ds(routed, extra)
+        if q is None:
+            return (ref, place.at[head]), (shared_ref.at[at], place.at[tail])
+        return (ref.at[:, q], place.at[head, q]), (shared_ref.at[at, q], place.at[tail, q])
+
+    def w_parts(k):
+        if k == 0:
+            return own_parts(gate_ref, s_gate_ref, wg.at[tp])
+        if k == 1:
+            return own_parts(up_ref, s_up_ref, wu.at[tp])
+        return own_parts(down_ref, s_down_ref, wd.at[tp], cols(k - 2))
+
+    def w_copy(k, by, way, refs=None):
         if way < 2:
             target = (me, tp + nc if way == 0 else tp - nc)
         else:
             target = (me, y * nc + (c + way - 1) % nc)
         owner = by * nc + c
-        src, dst = w_refs(k, owner, own)
+        src, dst = (w_place(k, owner), w_place(k, owner)) if refs is None else refs
         return pltpu.make_async_remote_copy(
             src_ref=src,
             dst_ref=dst,
@@ -103,21 +115,46 @@
         )
 
     def w_wait(k, owner):
-        src, dst = w_refs(k, owner, True)
         pltpu.make_async_remote_copy(
-            src_ref=src, dst_ref=dst, send_sem=w_send.at[0, 0, 0], recv_sem=w_recv.at[k, owner],
-            device_id=(me, tp), device_id_type=MESH,
+            src_ref=w_place(k, owner), dst_ref=w_place(k, owner), send_sem=w_send.at[0, 0, 0],
+            recv_sem=w_recv.at[k, owner], device_id=(me, tp), device_id_type=MESH,
         ).wait_recv()
 
-    def side_copy(j):
+    def side_source(ref, to):
+        if len(ref.shape) == 3:
+            return ref.at[to]
+        return ref.at[:, pl.ds(pl.multiple_of(to * side_cols, side_cols), side_cols)]
+
+    def side_copy(j, p):
         to = (me + j) % n_ep
         return pltpu.make_async_remote_copy(
-            src_ref=side_ref.at[to],
-            dst_ref=side.at[me],
+            src_ref=side_source((side_in_ref, side_out_ref)[p], to),
+            dst_ref=side.at[p * n_ep + me],
             send_sem=side_send.at[j],
             recv_sem=side_recv.at[me],
             device_id=(to, tp),
             device_id_type=MESH,
+        )
+
+    def side_each(act):
+        for p in range(nc):
+
+            @pl.when(c == p)
+            def _():
+                for j in range(1, n_ep):
+                    act(side_copy(j, p))
+
+    def side_own(p):
+        return pltpu.make_async_copy(
+            side_source((side_in_ref, side_out_ref)[p], me), side.at[p * n_ep + me],
+            local_sem.at[3],
+        )
+
+    def swap_copy():
+        half = side.at[pl.ds(c * n_ep, n_ep)]
+        return pltpu.make_async_remote_copy(
+            src_ref=half, dst_ref=half, send_sem=swap_send, recv_sem=swap_recv,
+            device_id=(me, y * nc + 1 - c), device_id_type=MESH,
         )
 
     def each_own(copy_of, at, last, ways, act):
@@ -165,12 +202,12 @@
 
     def tok_forward(step, act, arrive):
         each_forward(
-            lambda b, way: tok_copy(b, way, False), None, z, nz - 1, tok_ways, step, act, arrive
+            lambda b, way: tok_copy(b, way), None, z, nz - 1, tok_ways, step, act, arrive
         )
 
     def w_forward(k, step, act, arrive):
         each_forward(
-            lambda b, way: w_copy(k, b, way, False), None, y, ny - 1, w_ways, step, act, arrive
+            lambda b, way: w_copy(k, b, way), None, y, ny - 1, w_ways, step, act, arrive
         )
 
     def w_gathered(k):
@@ -182,35 +219,59 @@
             for by in range(ny):
                 w_wait(k, by * nc + (c + j) % nc)
 
-    each_own(lambda way: tok_copy(z, way, True), z, nz - 1, tok_ways, start)
     for k in range(pieces):
-        each_own(lambda way: w_copy(k, y, way, True), y, ny - 1, w_ways, start)
-    for j in range(1, n_ep):
-        side_copy(j).start()
-    tok[tok_rows(z, x)] = payload_ref[...]
-    wg[tp] = gate_ref[...]
-    wu[tp] = up_ref[...]
-    wd[tp] = down_ref[...]
-    side[me] = side_ref[me]
+        for refs in w_parts(k):
+            each_own(lambda way: w_copy(k, y, way, refs), y, ny - 1, w_ways, start)
+    whole_down = own_parts(down_ref, s_down_ref, wd.at[tp])
+    for n, parts in enumerate((w_parts(0), w_parts(1), whole_down)):
+        for src, dst in parts:
+            pltpu.make_async_copy(src, dst, local_sem.at[n]).start()
+
+    for p in range(nc):
+        pl.when(c == p)(lambda: side_own(p).start())
+
+    values = tokens_ref[...].astype(jnp.float32)
+    scale_inv = lax.rsqrt(jnp.mean(values * values, axis=-1, keepdims=True) + norm_eps)
+    normed = (values * scale_inv * gain_ref[...]).astype(jnp.bfloat16)
+    mine = tok_rows(z, x)
+    tok[mine, :width] = normed
+    gated = normed.astype(jnp.float32) * side_gate_ref[...].astype(jnp.float32)
+    opening = 1.0 / (1.0 + jnp.exp(-jnp.sum(gated, axis=-1, keepdims=True)))
+    lane = lax.broadcasted_iota(jnp.int32, (rows, 128), 1)
+    first = lane % 64
+    aux = jnp.where(first == experts_all, opening, 0.0)
+    for k in range(ids_ref.shape[1]):
+        aux = aux + jnp.where(first == ids_ref[:, k : k + 1], route_ref[:, k : k + 1], 0.0)
+    high = aux.astype(jnp.bfloat16)
+    low = (aux - high.astype(jnp.float32)).astype(jnp.bfloat16)
+    tok[mine, width:] = jnp.where(
+        lane < 64, high.astype(jnp.float32), low.astype(jnp.float32)
+    ).astype(jnp.bfloat16)
+    each_own(lambda way: tok_copy(z, way), z, nz - 1, tok_ways, start)
 
     def arrive_tok(b):
         tok_wait(b, x)
 
     for step in range(1, nz):
         tok_forward(step, start, arrive_tok)
+        if step == 1:
+            side_each(start)
         if step == nz - 2:
             w_gathered(0)
     w_gathered(1)
     w_across(0)
     w_across(1)
-    for j in range(1, n_ep):
-        b = (me + j) % n_ep
-        pltpu.make_async_remote_copy(
-            src_ref=side_ref.at[b], dst_ref=side.at[b], send_sem=side_send.at[0],
-            recv_sem=side_recv.at[b], device_id=(me, tp), device_id_type=MESH,
-        ).wait_recv()
+    for n, place in enumerate((wg, wu, wd)):
+        pltpu.make_async_copy(place.at[tp], place.at[tp], local_sem.at[n]).wait()
 
     tile = 2 * rows
+
+    def column(at, n):
+        aux = tok[at, width:].astype(jnp.float32)
+        lane = lax.broadcasted_iota(jnp.int32, aux.shape, 1)
+        hit = jnp.logical_or(lane == n, lane == n + 64)
+        return jnp.sum(jnp.where(hit, aux, 0.0), axis=1, keepdims=True)
+
     for j in range(nx):
         bx = (x + j) % nx
         if j:
@@ -226,27 +287,44 @@
             up_part = lax.dot_general(
                 a, wu[...].reshape(n_tp * part, width), NT, preferred_element_type=jnp.float32
             )
-            aux = tok[at, width:].astype(jnp.float32)
-            lane = lax.broadcasted_iota(jnp.int32, aux.shape, 1)
-
-            def column(n):
-                hit = jnp.logical_or(lane == n, lane == n + 64)
-                return jnp.sum(jnp.where(hit, aux, 0.0), axis=1, keepdims=True)
-
             scale = mask_ref[local_experts : local_experts + 1, :]
             for e in range(local_experts):
-                scale = scale + column(me * local_experts + e) * mask_ref[e : e + 1, :]
+                scale = scale + column(at, me * local_experts + e) * mask_ref[e : e + 1, :]
             hidden[at] = (silu(gate_part) * up_part * scale).astype(jnp.bfloat16)
-            side_part = jnp.dot(
-                a, side[:, 0].reshape(width, side.shape[3]), preferred_element_type=jnp.float32
-            )
-            side_hid[at] = (silu(side_part) * column(experts_all)).astype(jnp.bfloat16)
             return carry
 
         lax.fori_loop(0, nz * rows // tile, hidden_tile, 0)
+        if j == 0:
+            for p in range(nc):
+                pl.when(c == p)(lambda: side_own(p).wait())
+            for d in range(1, n_ep):
+                at = (me + d) % n_ep
+                block = side.at[c * n_ep + at]
+                pltpu.make_async_remote_copy(
+                    src_ref=block, dst_ref=block, send_sem=side_send.at[0],
+                    recv_sem=side_recv.at[at], device_id=(me, tp), device_id_type=MESH,
+                ).wait_recv()
+            swap_copy().start()
+
+    other = side.at[pl.ds((1 - c) * n_ep, n_ep)]
+    pltpu.make_async_remote_copy(
+        src_ref=other, dst_ref=other, send_sem=swap_send, recv_sem=swap_recv,
+        device_id=(me, tp), device_id_type=MESH,
+    ).wait_recv()
+
+    def side_tile(i, carry):
+        at = pl.ds(pl.multiple_of(i * tile, rows), tile)
+        side_part = jnp.dot(
+            tok[at, :width], side[:n_ep].reshape(width, side_cols),
+            preferred_element_type=jnp.float32,
+        )
+        side_hid[at] = (silu(side_part) * column(at, experts_all)).astype(jnp.bfloat16)
+        return carry
+
+    lax.fori_loop(0, n_ep * rows // tile, side_tile, 0)
 
     def x_copy(q, j, bz):
-        block = pl.ds(bz * rows, rows)
+        block = pl.ds(pl.multiple_of(bz * rows, rows), rows)
         return pltpu.make_async_remote_copy(
             src_ref=xs.at[q, j - 1, block],
             dst_ref=xr.at[q, j - 1, block],
@@ -272,7 +350,7 @@
 
     def multiply(q):
         down = wd[:, :, cols(q)].reshape(n_tp * part, piece)
-        side_down = side[pl.ds(q * blocks_per, blocks_per), 1].reshape(piece, side.shape[3])
+        side_down = side[pl.ds(n_ep + q * blocks_per, blocks_per)].reshape(piece, side_cols)
         for j in list(range(1, nx)) + [0]:
             at = pl.ds(pl.multiple_of((x + j) % nx * nz * rows, rows), nz * rows)
             value = jnp.dot(hidden[at], down, preferred_element_type=jnp.float32)
@@ -281,8 +359,9 @@
             )
             if j:
                 xs[q, j - 1] = value.astype(jnp.bfloat16)
-                for bz in range(nz):
-                    x_copy(q, j, bz).start()
+                for k in range(nz):
+                    far = (1 - z * 2 // nz) * (nz - 1 - k) + z * 2 // nz * k
+                    x_copy(q, j, far).start()
             else:
                 acc[q] = value
 
@@ -323,9 +402,18 @@
 
             l_copy(q, dz).start()
 
-        for k in range(nz - 1):
-            pl.when(z < nz - 1 - k)(functools.partial(right, nz - 1 - k))
-            pl.when(z > k)(functools.partial(left, k))
+        @pl.when(z * 2 < nz)
+        def _():
+            for k in range(nz - 1):
+                pl.when(z < nz - 1 - k)(functools.partial(right, nz - 1 - k))
+                pl.when(z > k)(functools.partial(left, k))
+
+        @pl.when(z * 2 >= nz)
+        def _():
+            for k in range(nz - 1):
+                pl.when(z > k)(functools.partial(left, k))
+                pl.when(z < nz - 1 - k)(functools.partial(right, nz - 1 - k))
+
         acc[q, pl.ds(0, rows)] = own(z)
 
     def settle(q):
@@ -351,15 +439,15 @@
     for q in range(chunks):
         settle(q)
 
-    each_own(lambda way: tok_copy(z, way, True), z, nz - 1, tok_ways, finish)
+    each_own(lambda way: tok_copy(z, way), z, nz - 1, tok_ways, finish)
     for step in range(1, nz):
         tok_forward(step, finish, nothing)
     for k in range(pieces):
-        each_own(lambda way: w_copy(k, y, way, True), y, ny - 1, w_ways, finish)
+        each_own(lambda way: w_copy(k, y, way), y, ny - 1, w_ways, finish)
         for step in range(1, ny):
             w_forward(k, step, finish, nothing)
-    for j in range(1, n_ep):
-        side_copy(j).wait_send()
+    side_each(finish)
+    swap_copy().wait_send()
     for q in range(chunks):
         for j in range(1, nx):
             for bz in range(nz):
@@ -386,42 +474,33 @@
     side_out,
     side_gate,
 ):
-    normed = normalize(tokens, norm_gain)
-    tok_count, width = normed.shape
+    tok_count, width = tokens.shape
     n_ep, n_tp = lax.axis_size("ep"), lax.axis_size("tp")
     nz, ny = n_ep // nx, n_tp // nc
     me = lax.axis_index("ep")
     local_experts, ff_part, _ = expert_gate.shape
+    routed = local_experts * ff_part
     experts_all = n_ep * local_experts
     shared_rows = shared_gate.shape[0] // n_ep
     side_rows, side_all = side_in.shape
     side_cols = side_all // n_ep
-    chunks = 4
+    chunks = 8
     piece = width // chunks
-
-    named = expert_ids[:, :, None] == jnp.arange(experts_all, dtype=jnp.int32)
-    dense = jnp.sum(jnp.where(named, route_weights[:, :, None], 0.0), axis=1)
-    opening = jax.nn.sigmoid(jnp.dot(normed, side_gate, preferred_element_type=jnp.float32))
-    aux = jnp.concatenate([dense, opening[:, None]], axis=1)
-    aux = jnp.pad(aux, ((0, 0), (0, 64 - aux.shape[1])))
-    high = lax.reduce_precision(aux, 8, 7)
-    payload = jnp.concatenate(
-        [normed, high.astype(jnp.bfloat16), (aux - high).astype(jnp.bfloat16)], axis=1
-    )
-
-    used = local_experts * ff_part + shared_rows
-    part = -(-used // 16) * 16
-
-    def pack(expert_part, shared_part):
-        own = lax.dynamic_slice_in_dim(shared_part, me * shared_rows, shared_rows, 0)
-        own = jnp.pad(own, ((0, part - used), (0, 0)))
-        return jnp.concatenate([expert_part.reshape(local_experts * ff_part, width), own], axis=0)
-
-    both = jnp.stack([side_in, side_out]).reshape(2, side_rows, n_ep, side_cols)
-    both = both.transpose(2, 0, 1, 3)
-    place = jnp.arange(n_tp * part, dtype=jnp.int32) % part // ff_part
-    place = jnp.minimum(place, local_experts)
-    mask = (place[None, :] == jnp.arange(local_experts + 1)[:, None]).astype(jnp.float32)
+    part = routed + -(-shared_rows // 16) * 16
+
+    def shared_part(array):
+        if shared_rows % 16 == 0:
+            return array
+        own = lax.dynamic_slice_in_dim(array, me * shared_rows, shared_rows, 0)
+        return jnp.pad(own, ((0, part - routed - shared_rows), (0, 0)))
+
+    def side_part(array):
+        if side_cols % 128 == 0:
+            return array
+        return array.reshape(side_rows, n_ep, side_cols).transpose(1, 0, 2)
+
+    place = np.minimum(np.arange(n_tp * part) % part // ff_part, local_experts)
+    mask = (place[None, :] == np.arange(local_experts + 1)[:, None]).astype(np.float32)
 
     bf16, f32 = jnp.bfloat16, jnp.float32
     dma = pltpu.SemaphoreType.DMA
@@ -429,14 +508,15 @@
     return pl.pallas_call(
         functools.partial(kernel, dims),
         out_shape=jax.ShapeDtypeStruct((tok_count, width), bf16),
-        in_specs=[pl.BlockSpec(memory_space=pltpu.VMEM)] * 6,
+        in_specs=[pl.BlockSpec(memory_space=pltpu.VMEM)] * 6
+        + [pl.BlockSpec(memory_space=pl.ANY)] * 8,
         out_specs=pl.BlockSpec(memory_space=pltpu.VMEM),
         scratch_shapes=[
-            pltpu.VMEM((n_ep * tok_count, payload.shape[1]), bf16),
+            pltpu.VMEM((n_ep * tok_count, width + 128), bf16),
             pltpu.VMEM((n_tp, part, width), bf16),
             pltpu.VMEM((n_tp, part, width), bf16),
             pltpu.VMEM((n_tp, part, width), bf16),
-            pltpu.VMEM((n_ep, 2, side_rows, side_cols), bf16),
+            pltpu.VMEM((2 * n_ep, side_rows, side_cols), bf16),
             pltpu.VMEM((n_ep * tok_count, n_tp * part), bf16),
             pltpu.VMEM((n_ep * tok_count, side_cols), bf16),
             pltpu.VMEM((chunks, nz * tok_count, piece), f32),
@@ -450,6 +530,9 @@
             dma((2 + chunks, n_tp)),
             dma((n_ep,)),
             dma((n_ep,)),
+            dma,
+            dma,
+            dma((4,)),
             dma((chunks, nx - 1, nz)),
             dma((chunks, nx - 1, nz)),
             dma((chunks, nz)),
@@ -461,8 +544,12 @@
             collective_id=0, has_side_effects=True, vmem_limit_bytes=63000 * 1024
         ),
         name="layer",
-    )(payload, pack(expert_gate, shared_gate), pack(expert_up, shared_up),
-      pack(expert_down, shared_down), both, mask)
+    )(
+        tokens, norm_gain[None, :], expert_ids, route_weights, side_gate[None, :], mask,
+        expert_gate.reshape(routed, width), expert_up.reshape(routed, width),
+        expert_down.reshape(routed, width), shared_part(shared_gate), shared_part(shared_up),
+        shared_part(shared_down), side_part(side_in), side_part(side_out),
+    )
 
 
 def solution(mesh):

time: 190 us -> 154 us (0.81)
  Pallas kernels: 175 us -> 149 us
  other arithmetic: 7.32 us -> 0 us
  local copies, waits for them, and re-layouts: 7.33 us -> 4.68 us
    pallas_call x1, Pallas kernels: 175 us -> 149 us  [body(): pl.pallas_call(functools.partial(kernel, dims), out_shape=jax.ShapeDtypeS...]
    concatenate x4 -> x0, other arithmetic: 3.25 us -> none  [the longest x3 3.24 us: pack(): jnp.concatenate([expert_part.reshape(local_experts * ff_part, width), own...]
    reduce_sum x2 -> x0, other arithmetic: 2.09 us -> none  [the longest x1 1.35 us: normalize(): jnp.mean(values * values, axis=-1, keepdims=True) + norm_eps]
    unnamed x20 -> x9, local copies, waits for them, and re-layouts: 4.78 us -> 4.09 us
where the time goes in v3:
time: 154 us
  Pallas kernels  149 us (97%)
  local copies, waits for them, and re-layouts  4.68 us (3%)
    pallas_call x1, Pallas kernels, body(): pl.pallas_call(functools.partial(kernel, dims), out_shape=jax.ShapeDtypeS...  149 us
    unnamed x9, local copies, waits for them, and re-layouts  4.09 us

profile of v3, /device:TPU:0, one launch (start us, length us, event | category | flops | bytes accessed | tf_op | source)
XLA Modules:
  0.0 154.1 jit_solution(4783127235363681520)
XLA Ops:
  0.0 0.0 copy-start.2
  0.0 0.0 copy-start
  0.0 0.7 copy-done.2
  0.7 0.6 broadcast_in_dim.7.side_gate_ref
  1.3 0.0 copy-done
  1.3 0.0 copy-start.1
  1.3 0.7 copy.15.ids_ref
  2.0 0.0 copy-done.1
  2.0 0.7 copy.16.route_ref
  2.8 149.4 %layer.1 = bf16[144,2048]{1,0:T(8,128)(2,1)} custom-call(bf16[144,2048]{1,0:T(8,128)(2,1)} %tokens_ref.1, f32[1,2048]{1,0:T(1,128)} %bitcast.7, s32[144,8]{1,0:T(8,128)} %copy.15.ids_ref, f32[144,8]{1,0:T(8,128)} %copy.16.route_ref, bf16[1,2048]{1,0:T(2,128)(2,1)} %broadcast_in_dim.7.side_gate_ref, f32[3,1088]{1,0:T(4,128)} %constant.2.clone.mask_ref, ...), custom_call_target="tpu_custom_call" | custom-call | tf_op jit(solution)/shard_map/layer/pallas_call | solution.py:508
  152.1 1.9 %copy.18 = bf16[144,2048]{1,0:T(8,128)(2,1)} copy(bf16[144,2048]{1,0:T(8,128)(2,1)} %layer.1) | data formatting | bytes 1179648
Async XLA Ops:
  0.0 0.7 copy-start.2
  0.0 1.3 copy-start
  1.3 0.7 copy-start.1

commit v4 on v3

--- a/solution.py
+++ b/solution.py
@@ -274,12 +274,13 @@
 
     for j in range(nx):
         bx = (x + j) % nx
-        if j:
-            for bz in range(nz):
-                tok_wait(bz, bx)
 
         def hidden_tile(i, carry):
-            at = pl.ds(pl.multiple_of(bx * nz * rows + i * tile, rows), tile)
+            pair = (z // 2 + i) % (nz // 2)
+            if j:
+                tok_wait(2 * pair, bx)
+                tok_wait(2 * pair + 1, bx)
+            at = pl.ds(pl.multiple_of(bx * nz * rows + pair * tile, rows), tile)
             a = tok[at, :width]
             gate_part = lax.dot_general(
                 a, wg[...].reshape(n_tp * part, width), NT, preferred_element_type=jnp.float32
@@ -293,7 +294,7 @@
             hidden[at] = (silu(gate_part) * up_part * scale).astype(jnp.bfloat16)
             return carry
 
-        lax.fori_loop(0, nz * rows // tile, hidden_tile, 0)
+        lax.fori_loop(0, nz // 2, hidden_tile, 0)
         if j == 0:
             for p in range(nc):
                 pl.when(c == p)(lambda: side_own(p).wait())

time: 154 us -> 151 us (0.981)
  Pallas kernels: 149 us -> 146 us
    pallas_call x1, Pallas kernels: 149 us -> 146 us  [body(): pl.pallas_call(functools.partial(kernel, dims), out_shape=jax.ShapeDtypeS...]
where the time goes in v4:
time: 151 us
  Pallas kernels  146 us (97%)
  local copies, waits for them, and re-layouts  4.68 us (3%)
    pallas_call x1, Pallas kernels, body(): pl.pallas_call(functools.partial(kernel, dims), out_shape=jax.ShapeDtypeS...  146 us
    unnamed x9, local copies, waits for them, and re-layouts  4.09 us

profile of v4, /device:TPU:0, one launch (start us, length us, event | category | flops | bytes accessed | tf_op | source)
XLA Modules:
  0.0 150.8 jit_solution(10107020644007738608)
XLA Ops:
  0.0 0.0 copy-start.2
  0.0 0.0 copy-start
  0.0 0.7 copy-done.2
  0.7 0.6 broadcast_in_dim.7.side_gate_ref
  1.3 0.0 copy-done
  1.3 0.0 copy-start.1
  1.3 0.7 copy.15.ids_ref
  2.0 0.0 copy-done.1
  2.0 0.7 copy.16.route_ref
  2.8 146.1 %layer.1 = bf16[144,2048]{1,0:T(8,128)(2,1)} custom-call(bf16[144,2048]{1,0:T(8,128)(2,1)} %tokens_ref.1, f32[1,2048]{1,0:T(1,128)} %bitcast.7, s32[144,8]{1,0:T(8,128)} %copy.15.ids_ref, f32[144,8]{1,0:T(8,128)} %copy.16.route_ref, bf16[1,2048]{1,0:T(2,128)(2,1)} %broadcast_in_dim.7.side_gate_ref, f32[3,1088]{1,0:T(4,128)} %constant.2.clone.mask_ref, ...), custom_call_target="tpu_custom_call" | custom-call | tf_op jit(solution)/shard_map/layer/pallas_call | solution.py:509
  148.8 1.9 %copy.18 = bf16[144,2048]{1,0:T(8,128)(2,1)} copy(bf16[144,2048]{1,0:T(8,128)(2,1)} %layer.1) | data formatting | bytes 1179648
Async XLA Ops:
  0.0 0.7 copy-start.2
  0.0 1.3 copy-start
  1.3 0.7 copy-start.1
